TPU v7x, 32 devices: a whole 2x2x4 slice. The times are simulated.
32 devices in a mesh: fs: 8 (over z, x), tp: 4 (over y, core).
Axes of the slice: x: 2, y: 2, z: 4, core: 2. Of those that a mesh axis runs over, the one named last changes fastest.
Arguments:
- tokens: bfloat16 [2048, 2048], P('fs', 'tp'), may hold values from -6 to 6
- grad_out: bfloat16 [2048, 2048], P('fs', 'tp'), may hold values from -6 to 6
- up_weight: bfloat16 [2048, 4096], P('fs', 'tp'), may hold values from -0.125 to 0.125
- down_weight: bfloat16 [4096, 2048], P('tp', 'fs'), may hold values from -0.09375 to 0.09375
Outputs:
- input_grad: bfloat16 [2048, 2048], P('fs', 'tp')
- up_grad: float32 [2048, 4096], P('fs', 'tp')
- down_grad: float32 [4096, 2048], P('tp', 'fs')
- up_norms: float32 [2048], P('fs')
- down_norms: float32 [4096], P('tp')
All inputs are finite; a program needn't handle non-finite values.
Results may differ from a plain program's by a relative error of at most 0.015.
Values may be sent and summed in bfloat16 or wider, within the bound.
A program may use at most 64 MiB of HBM per device.

v0:
```python
import jax
import jax.numpy as jnp
from jax import lax
from jax.sharding import PartitionSpec as P


def on_device(tokens, grad_out, up_weight, down_weight):
    rows, cotan = (
        lax.all_gather(tokens, "tp", axis=1, tiled=True),
        lax.all_gather(grad_out, "tp", axis=1, tiled=True),
    )
    up_local = lax.all_gather(up_weight, "fs", axis=0, tiled=True)
    dact = lax.dot_general(
        cotan,
        lax.all_gather(down_weight, "fs", axis=1, tiled=True),
        (((1,), (1,)), ((), ())),
        preferred_element_type=jnp.float32,
    )
    pre = jnp.dot(rows, up_local, preferred_element_type=jnp.float32)
    relued = jnp.maximum(pre, 0.0)
    act = (relued * relued).astype(jnp.bfloat16)
    dpre = (dact * 2.0 * relued).astype(jnp.bfloat16)
    partial_sum = lax.dot_general(
        dpre, up_local, (((1,), (1,)), ((), ())), preferred_element_type=jnp.float32
    )
    rounded = lax.optimization_barrier(partial_sum.astype(jnp.bfloat16))
    input_grad = lax.psum_scatter(
        rounded.astype(jnp.float32).astype(jnp.bfloat16), "tp", scatter_dimension=1, tiled=True
    )
    cols = rows
    up_shard = lax.psum_scatter(
        lax.dot_general(
            cols, dpre, (((0,), (0,)), ((), ())), preferred_element_type=jnp.float32
        ).astype(jnp.bfloat16),
        "fs",
        scatter_dimension=0,
        tiled=True,
    ).astype(jnp.float32)
    cols = cotan
    down_flip = lax.psum_scatter(
        lax.dot_general(
            cols, act, (((0,), (0,)), ((), ())), preferred_element_type=jnp.float32
        ).astype(jnp.bfloat16),
        "fs",
        scatter_dimension=0,
        tiled=True,
    ).astype(jnp.float32)
    down_grad = down_flip.T
    up_norms = lax.psum(jnp.sum(up_shard * up_shard, axis=1), "tp")
    down_norms = lax.psum(jnp.sum(down_grad * down_grad, axis=1), "fs")
    return (input_grad, up_shard, down_grad, up_norms, down_norms)


def solution(mesh):
    return jax.shard_map(
        on_device,
        mesh=mesh,
        in_specs=(P("fs", "tp"), P("fs", "tp"), P("fs", "tp"), P("tp", "fs")),
        out_specs=(P("fs", "tp"), P("fs", "tp"), P("tp", "fs"), P("fs"), P("tp")),
        check_vma=False,
    )
```

profile of v0, /device:TPU:0, one launch (start us, length us, event | category | flops | bytes accessed | tf_op | source)
XLA Modules:
  0.0 419.1 jit_solution(4892946634751360285)
XLA Ops:
  7.2 0.7 all-gather.9.cloned.1.call-update
  7.9 0.7 all-gather.11.cloned.1.call-update
  8.7 0.7 all-gather.5.cloned.1.call-update
  9.4 0.5 all-gather.7.cloned.1.call-update
  10.0 0.0 reduce-scatter.6.cloned.1.call-start
  10.0 19.0 %all-gather.9.cloned.1.call-done = bf16[256,2048]{1,0:T(8,128)(2,1)} async-done(((bf16[256,512]{1,0:T(8,128)(2,1)}), bf16[256,2048]{1,0:T(8,128)(2,1)}) %all-gather.9.cloned.1.call-update) | async-done | bytes 1048592 | tf_op jit(solution)/shard_map/all_gather | solution.py:9
  29.0 74.9 %all-gather.11.cloned.1.call-done = bf16[2048,1024]{1,0:T(8,128)(2,1)} async-done(((bf16[256,1024]{1,0:T(8,128)(2,1)}), bf16[2048,1024]{1,0:T(8,128)(2,1)}) %all-gather.11.cloned.1.call-update) | async-done | bytes 4194320 | tf_op jit(solution)/shard_map/all_gather | solution.py:12
  103.9 3.8 convolution_maximum_fusion
  107.7 13.1 %all-gather.5.cloned.1.call-done = bf16[256,2048]{1,0:T(8,128)(2,1)} async-done(((bf16[256,512]{1,0:T(8,128)(2,1)}), bf16[256,2048]{1,0:T(8,128)(2,1)}) %all-gather.5.cloned.1.call-update) | async-done | bytes 1048592 | tf_op jit(solution)/shard_map/all_gather | solution.py:10
  120.8 76.6 %all-gather.7.cloned.1.call-done = bf16[1024,2048]{1,0:T(8,128)(2,1)} async-done(((bf16[1024,256]{1,0:T(8,128)(2,1)}), bf16[1024,2048]{1,0:T(8,128)(2,1)}) %all-gather.7.cloned.1.call-update) | async-done | bytes 4194320 | tf_op jit(solution)/shard_map/all_gather | solution.py:15
  197.3 3.8 fusion.1
  201.1 4.6 %convert_bitcast_fusion.1 = bf16[2048,1024]{0,1:T(8,128)(2,1)} fusion(bf16[256,1024]{1,0:T(8,128)(2,1)S(1)} %fusion.1, bf16[256,2048]{1,0:T(8,128)(2,1)} %all-gather.9.cloned.1.call-done), kind=kOutput, calls=%fused_computation.1 | convolution fusion | flops 1075838976 | bytes 5767168 | tf_op jit(solution)/shard_map/dot_general | solution.py:32
  205.8 0.0 reduce-scatter.8.cloned.1.call-start
  205.8 3.3 convert_bitcast_fusion
  209.1 0.0 reduce-scatter.4.cloned.1.call-start
  209.1 4.6 %convolution_convert_fusion = bf16[256,2048]{1,0:T(8,128)(2,1)} fusion(bf16[256,1024]{1,0:T(8,128)(2,1)S(1)} %fusion.1, bf16[2048,1024]{1,0:T(8,128)(2,1)} %all-gather.11.cloned.1.call-done), kind=kOutput, calls=%fused_computation.2 | convolution fusion | flops 1074266112 | bytes 5767168 | tf_op jit(solution)/shard_map/dot_general | solution.py:23
  213.7 79.1 %reduce-scatter.6.cloned.1.call-done = bf16[256,1024]{0,1:T(8,128)(2,1)} async-done(((bf16[2048,1024]{0,1:T(8,128)(2,1)}), bf16[256,1024]{0,1:T(8,128)(2,1)}) %reduce-scatter.6.cloned.1.call-update) | async-done | bytes 524304 | tf_op jit(solution)/shard_map/reduce_scatter | solution.py:31
  292.8 2.2 copy.9
  295.1 1.2 multiply_reduce_fusion.1
  296.3 6.7 %psum.14 = f32[256]{0:T(256)} all-reduce(f32[256]{0:T(256)S(1)} %multiply_reduce_fusion.1), channel_id=1, replica_groups=mesh['fs'=8,'tp'=4] {'tp'}, use_global_device_ids=true, to_apply=%region_4.0 | all-reduce | flops 256 | bytes 2048 | tf_op jit(solution)/shard_map/psum | solution.py:49
  303.0 81.7 %reduce-scatter.8.cloned.1.call-done = bf16[256,1024]{0,1:T(8,128)(2,1)} async-done(((bf16[2048,1024]{0,1:T(8,128)(2,1)}), bf16[256,1024]{0,1:T(8,128)(2,1)}) %reduce-scatter.8.cloned.1.call-update) | async-done | bytes 524304 | tf_op jit(solution)/shard_map/reduce_scatter | solution.py:40
  384.7 2.1 multiply_reduce_fusion
  386.8 20.6 %psum.15 = f32[1024]{0:T(1024)} all-reduce(f32[1024]{0:T(1024)S(1)} %get-tuple-element.10), channel_id=1, replica_groups=mesh['fs'=8,'tp'=4] {'fs'}, use_global_device_ids=true, to_apply=%region_6.0 | all-reduce | flops 1024 | bytes 8192 | tf_op jit(solution)/shard_map/psum | solution.py:50
  407.4 4.8 %reduce-scatter.4.cloned.1.call-done = bf16[256,512]{1,0:T(8,128)(2,1)} async-done(((bf16[256,2048]{1,0:T(8,128)(2,1)}), bf16[256,512]{1,0:T(8,128)(2,1)}) %reduce-scatter.4.cloned.1.call-update) | async-done | bytes 262160 | tf_op jit(solution)/shard_map/reduce_scatter | solution.py:27
  (9 shorter events, 0.2 us)
Async XLA Ops:
  7.2 21.8 %all-gather.9.cloned.1.call-start = ((), (), s32[]{:S(2)}) async-start(), calls=%async_computation.5 | async-start | bytes 1310720 | tf_op jit(solution)/shard_map/all_gather | solution.py:9
  7.9 96.0 %all-gather.11.cloned.1.call-start = ((), (), s32[]{:S(2)}) async-start(), calls=%async_computation.6 | async-start | bytes 4718592 | tf_op jit(solution)/shard_map/all_gather | solution.py:12
  8.6 112.1 %all-gather.5.cloned.1.call-start = ((), (), s32[]{:S(2)}) async-start(), calls=%async_computation.3 | async-start | bytes 1310720 | tf_op jit(solution)/shard_map/all_gather | solution.py:10
  9.4 188.0 %all-gather.7.cloned.1.call-start = ((), (), s32[]{:S(2)}) async-start(), calls=%async_computation.4 | async-start | bytes 4718592 | tf_op jit(solution)/shard_map/all_gather | solution.py:15
  10.0 282.9 %reduce-scatter.6.cloned.1.call-start = ((), (), s32[]{:S(2)}) async-start(), calls=%async_computation.8 | async-start | bytes 4718592 | tf_op jit(solution)/shard_map/reduce_scatter | solution.py:31
  201.1 4.7 %copy-start = (bf16[256,2048]{1,0:T(8,128)(2,1)S(1)}, bf16[256,2048]{1,0:T(8,128)(2,1)}, u32[]{:S(2)}) copy-start(bf16[256,2048]{1,0:T(8,128)(2,1)} %all-gather.5.cloned.1.call-done) | copy-start | bytes 3145732
  205.8 179.0 %reduce-scatter.8.cloned.1.call-start = ((), (), s32[]{:S(2)}) async-start(), calls=%async_computation.9 | async-start | bytes 4718592 | tf_op jit(solution)/shard_map/reduce_scatter | solution.py:40
  209.1 203.2 %reduce-scatter.4.cloned.1.call-start = ((), (), s32[]{:S(2)}) async-start(), calls=%async_computation.7 | async-start | bytes 1310720 | tf_op jit(solution)/shard_map/reduce_scatter | solution.py:27
Sparse Core Ops, SparseCore 0:
  9.5 19.4 all-gather.8
  31.1 72.7 all-gather.10
  105.5 15.2 all-gather.4
  122.7 74.6 all-gather.6
  205.9 86.9 reduce-scatter.5
  296.3 88.3 reduce-scatter.7
  387.8 24.4 reduce-scatter.3
where the time goes:
time: 419 us
  waiting for transfers between devices  352 us (84%)
  blocking collectives  27.4 us (7%)
  matrix products  20 us (5%)
  between operations  14.2 us (3%)
    reduce_scatter x1, waiting for transfers between devices, on_device(): lax.psum_scatter(lax.dot_general(cols, act, (((0,), (0,)), ((), ())), pre...  81.7 us
    reduce_scatter x1, waiting for transfers between devices, on_device(): lax.psum_scatter(lax.dot_general(cols, dpre, (((0,), (0,)), ((), ())), pr...  79.1 us
    all_gather x1, waiting for transfers between devices, on_device(): lax.all_gather(down_weight, 'fs', axis=1, tiled=True)  76.6 us
    all_gather x1, waiting for transfers between devices, on_device(): up_local = lax.all_gather(up_weight, 'fs', axis=0, tiled=True)  74.9 us
    psum x1, blocking collectives, on_device(): down_norms = lax.psum(jnp.sum(down_grad * down_grad, axis=1), 'fs')  20.6 us
    all_gather x1, waiting for transfers between devices, on_device(): lax.all_gather(tokens, 'tp', axis=1, tiled=True)  19 us
    all_gather x1, waiting for transfers between devices, on_device(): lax.all_gather(grad_out, 'tp', axis=1, tiled=True)  13.1 us
  transfers between devices with their start and end apart: 7, of which 7 were waited for; matrix products, arithmetic and copies ran while one was open for 4% of the time, Pallas kernels for 0%

commit v1 on v0

v1 whole, which is shorter than its diff:
```python
import functools

import jax
import jax.numpy as jnp
from jax import lax
from jax.experimental import pallas as pl
from jax.experimental.pallas import tpu as pltpu
from jax.sharding import PartitionSpec as P

BF = jnp.bfloat16
F32 = jnp.float32


def on_device(tokens, grad_out, up_weight, down_weight):
    rows, cotan = (
        lax.all_gather(tokens, "tp", axis=1, tiled=True),
        lax.all_gather(grad_out, "tp", axis=1, tiled=True),
    )
    up_local = lax.all_gather(up_weight, "fs", axis=0, tiled=True)
    dact = lax.dot_general(
        cotan,
        lax.all_gather(down_weight, "fs", axis=1, tiled=True),
        (((1,), (1,)), ((), ())),
        preferred_element_type=F32,
    )
    pre = jnp.dot(rows, up_local, preferred_element_type=F32)
    relued = jnp.maximum(pre, 0.0)
    act = (relued * relued).astype(BF)
    dpre = (dact * 2.0 * relued).astype(BF)
    partial_sum = lax.dot_general(
        dpre, up_local, (((1,), (1,)), ((), ())), preferred_element_type=F32
    )
    rounded = lax.optimization_barrier(partial_sum.astype(BF))
    input_grad = lax.psum_scatter(rounded, "tp", scatter_dimension=1, tiled=True)
    up_shard = lax.psum_scatter(
        lax.dot_general(
            rows, dpre, (((0,), (0,)), ((), ())), preferred_element_type=F32
        ).astype(BF),
        "fs",
        scatter_dimension=0,
        tiled=True,
    ).astype(F32)
    down_flip = lax.psum_scatter(
        lax.dot_general(
            cotan, act, (((0,), (0,)), ((), ())), preferred_element_type=F32
        ).astype(BF),
        "fs",
        scatter_dimension=0,
        tiled=True,
    ).astype(F32)
    down_grad = down_flip.T
    up_norms = lax.psum(jnp.sum(up_shard * up_shard, axis=1), "tp")
    down_norms = lax.psum(jnp.sum(down_grad * down_grad, axis=1), "fs")
    return (input_grad, up_shard, down_grad, up_norms, down_norms)


def dot(a, b, ca, cb, **kw):
    return lax.dot_general(a, b, (((ca,), (cb,)), ((), ())), preferred_element_type=F32, **kw)


def kernel(Z, tok, grd, upw, dnw, ig_o, ug_o, dg_o, un_o, dn_o,
           TG, UW, DW, ACT, DP, PO, PCs, PCr, PYs, PYr, PZs, PZr,
           GXs, GXr, GZs, GZr, NUs, NUr, NDs, NDr,
           ss, ls, wz, wx, tz, ty, tc, pc, py, pz, gx, gz, nu, nd):
    X = Y = C = 2
    TB, KB = tok.shape
    RB = upw.shape[0]
    HB = upw.shape[1] // Z
    FS, TP = Z * X, Y * C
    f = lax.axis_index("fs")
    t = lax.axis_index("tp")
    z, x = f // X, f % X
    y, c = t // C, t % C
    xn, yn, cn = 1 - x, 1 - y, 1 - c
    DX = {"fs": z * X + xn, "tp": t}
    DY = {"fs": f, "tp": yn * C + c}
    DC = {"fs": f, "tp": y * C + cn}

    def at_z(zz):
        return {"fs": zz * X + x, "tp": t}

    order = []
    for i in range(Z):
        o = jnp.int32(0)
        for zz in range(Z):
            near = sorted(range(Z), key=lambda q: (abs(q - zz), q))
            o = jnp.where(z == zz, near[i], o)
        order.append(o)

    def blk(i, n):
        return pl.ds(pl.multiple_of(i * n, n), n)

    sends = []

    def send(src, dst, rsem, dev, cond=None):
        d = pltpu.make_async_remote_copy(
            src_ref=src, dst_ref=dst, send_sem=ss.at[len(sends)], recv_sem=rsem,
            device_id=dev, device_id_type=pl.DeviceIdType.MESH)
        sends.append((d, cond))
        if cond is None:
            d.start()
        else:
            pl.when(cond)(d.start)

    def got(dst, rsem):
        pltpu.make_async_remote_copy(
            src_ref=dst, dst_ref=dst, send_sem=ss.at[0], recv_sem=rsem,
            device_id=DX, device_id_type=pl.DeviceIdType.MESH).wait_recv()

    bar = pltpu.get_barrier_semaphore()
    for p in range(1, FS):
        pl.semaphore_signal(bar, inc=1, device_id={"fs": (f + p) % FS, "tp": t},
                            device_id_type=pl.DeviceIdType.MESH)
    for p in range(1, TP):
        pl.semaphore_signal(bar, inc=1, device_id={"fs": f, "tp": (t + p) % TP},
                            device_id_type=pl.DeviceIdType.MESH)

    TK = (tok, grd)

    def tgr(a, o, k):
        return TG.at[a, blk(o, TB), blk(k, KB)]

    def w_src(a, zz):
        return upw.at[:, blk(zz, HB)] if a == 0 else dnw.at[blk(zz, HB), :]

    def w_dst(a, ff):
        return UW.at[blk(ff, RB), :] if a == 0 else DW.at[:, blk(ff, RB)]

    local = []
    for a in range(2):
        local.append(pltpu.make_async_copy(w_src(a, z), w_dst(a, f), ls.at[a]))
        local.append(pltpu.make_async_copy(TK[a], tgr(a, z, t), ls.at[2 + a]))
    for d in local:
        d.start()
    pl.semaphore_wait(bar, FS - 1 + TP - 1)

    for a in range(2):
        send(w_src(a, z), w_dst(a, f), wx.at[a, z], DX)
        send(TK[a], tgr(a, z, t), ty.at[a, z], DY)
        send(TK[a], tgr(a, z, t), tc.at[a, z, y], DC)
    for i in range(1, Z):
        for a in range(2):
            send(w_src(a, order[i]), w_dst(a, f), wz.at[a, z], at_z(order[i]))
    up_z = jnp.minimum(z + 1, Z - 1)
    dn_z = jnp.maximum(z - 1, 0)
    for a in range(2):
        send(TK[a], tgr(a, z, t), tz.at[a, z], at_z(up_z), z < Z - 1)
        send(TK[a], tgr(a, z, t), tz.at[a, z], at_z(dn_z), z > 0)

    def arrive(i):
        o = order[i]
        for a in range(2):
            r = tgr(a, o, t)
            got(r, tz.at[a, o])
            send(r, r, tz.at[a, o], at_z(up_z), (o < z) & (z < Z - 1))
            send(r, r, tz.at[a, o], at_z(dn_z), (o > z) & (z > 0))
            send(r, r, ty.at[a, o], DY)
            send(r, r, tc.at[a, o, y], DC)

    def yfwd(i):
        o = order[i]
        for a in range(2):
            r = tgr(a, o, yn * C + c)
            got(r, ty.at[a, o])
            send(r, r, tc.at[a, o, yn], DC)

    def ready(i):
        o = order[i]
        for a in range(2):
            for yy in range(Y):
                got(tgr(a, o, yy * C + cn), tc.at[a, o, yy])

    def hidden(i):
        r = blk(order[i], TB)
        pre = dot(TG[0, r, :], UW[...], 1, 0)
        dact = dot(TG[1, r, :], DW[...], 1, 1)
        relued = jnp.maximum(pre, 0.0)
        ACT[r, :] = (relued * relued).astype(BF)
        DP[r, :] = (dact * 2.0 * relued).astype(BF)

    def back(i):
        d = DP[blk(order[i], TB), :]
        for yy in range(Y):
            for cc, keep in ((cn, False), (c, True)):
                part = dot(d, UW[blk(yy * C + cc, KB), :], 1, 1)
                if keep:
                    PO[i, yy] = part.astype(BF)
                else:
                    PCs[i, yy] = part.astype(BF)
                    send(PCs.at[i, yy], PCr.at[i, yy], pc.at[i, yy], DC)

    def core_sum(i):
        for yy in range(Y):
            got(PCr.at[i, yy], pc.at[i, yy])
        PYs[i] = (PO[i, yn].astype(F32) + PCr[i, yn].astype(F32)).astype(BF)
        send(PYs.at[i], PYr.at[i], py.at[i], DY)

    def y_sum(i):
        got(PYr.at[i], py.at[i])
        s = PO[i, y].astype(F32) + PCr[i, y].astype(F32) + PYr[i].astype(F32)
        if i == 0:
            return s
        PZs[i] = s.astype(BF)
        send(PZs.at[i], PZr.at[z], pz.at[z], at_z(order[i]))

    def grads(a, ff):
        if a == 0:
            return dot(TG[0, :, blk(ff, RB)], DP[...], 0, 0)
        return dot(ACT[...], TG[1, :, blk(ff, RB)], 0, 0)

    for i in range(1, Z):
        o = order[i]
        for a in range(2):
            r = w_dst(a, o * X + x)
            got(r, wz.at[a, o])
            send(r, r, wx.at[a, o], DX)
    yfwd(0)
    arrive(1)
    for d in local:
        d.wait()
    for i in range(Z):
        for a in range(2):
            got(w_dst(a, order[i] * X + xn), wx.at[a, order[i]])
    for i in range(Z):
        ready(i)
        hidden(i)
        if i + 1 < Z:
            back(i)
            yfwd(i + 1)
        if i + 2 < Z:
            arrive(i + 2)
        if i >= 1:
            core_sum(i - 1)
        if i >= 2 and i + 1 < Z:
            y_sum(i - 1)

    far = list(range(Z - 1, -1, -1))
    for i in far:
        for a in range(2):
            GXs[a, i] = grads(a, order[i] * X + xn).astype(BF)
            send(GXs.at[a, i], GXr.at[a, i], gx.at[a, i], DX)
    back(Z - 1)
    if Z > 2:
        y_sum(Z - 2)
    for i in far:
        o = order[i]
        for a in range(2):
            g = grads(a, o * X + x)
            got(GXr.at[a, i], gx.at[a, i])
            g = g + GXr[a, i].astype(F32)
            if i:
                GZs[a, i] = g.astype(BF)
                send(GZs.at[a, i], GZr.at[a, z], gz.at[a, z], at_z(o))
            elif a == 0:
                ug_o[:, blk(o, HB)] = g
            else:
                dg_o[blk(o, HB), :] = g
        if i == Z - 1:
            core_sum(Z - 1)
    y_sum(Z - 1)
    total = y_sum(0)
    for i in range(1, Z):
        got(PZr.at[order[i]], pz.at[order[i]])
        total = total + PZr[order[i]].astype(F32)
    ig_o[...] = total.astype(BF)

    for i in range(1, Z):
        o = order[i]
        for a in range(2):
            got(GZr.at[a, o], gz.at[a, o])
        ug_o[:, blk(o, HB)] = GZr[0, o].astype(F32)
        dg_o[blk(o, HB), :] = GZr[1, o].astype(F32)

    hi = dict(precision=lax.Precision.HIGHEST)
    g = ug_o[...]
    nu_mine = dot(jnp.ones((8, g.shape[1]), F32), g * g, 1, 1, **hi)
    NUs[...] = nu_mine
    for p in range(1, TP):
        send(NUs, NUr.at[t], nu.at[t], {"fs": f, "tp": (t + p) % TP})
    g = dg_o[...]
    nd_mine = dot(jnp.ones((8, g.shape[1]), F32), g * g, 1, 1, **hi)
    NDs[...] = nd_mine
    for p in range(1, FS):
        send(NDs, NDr.at[f], nd.at[f], {"fs": (f + p) % FS, "tp": t})
    NUr[t] = nu_mine
    NDr[f] = nd_mine
    for p in range(1, TP):
        q = (t + p) % TP
        got(NUr.at[q], nu.at[q])
    for p in range(1, FS):
        q = (f + p) % FS
        got(NDr.at[q], nd.at[q])
    un_o[...] = sum(NUr[q] for q in range(TP))
    dn_o[...] = sum(NDr[q] for q in range(FS))

    for d, cond in sends:
        if cond is None:
            d.wait_send()
        else:
            pl.when(cond)(d.wait_send)


def fused(Z, tokens, grad_out, up_weight, down_weight):
    TB, KB = tokens.shape
    RB, HL = up_weight.shape
    HB, X, Y, C = HL // Z, 2, 2, 2
    FS, TP = Z * X, Y * C
    D, T = KB * TP, TB * Z
    V, S = pltpu.VMEM, pltpu.SemaphoreType.DMA
    any_ = pl.BlockSpec(memory_space=pl.ANY)
    vm = pl.BlockSpec(memory_space=pltpu.VMEM)
    n_sends = 2 * 3 + 2 * (Z - 1) + 4 + 8 * (Z - 1) + 2 * Z + 2 * (Z - 1)
    n_sends += 2 * Z + Z + Z - 1 + 2 * Z + 2 * (Z - 1) + TP - 1 + FS - 1
    outs = pl.pallas_call(
        functools.partial(kernel, Z),
        out_shape=(
            jax.ShapeDtypeStruct((TB, KB), BF),
            jax.ShapeDtypeStruct((RB, HL), F32),
            jax.ShapeDtypeStruct((HL, RB), F32),
            jax.ShapeDtypeStruct((8, RB), F32),
            jax.ShapeDtypeStruct((8, HL), F32),
        ),
        in_specs=[any_] * 4,
        out_specs=[vm] * 5,
        scratch_shapes=[
            V((2, T, D), BF), V((D, HB), BF), V((HB, D), BF), V((T, HB), BF), V((T, HB), BF),
            V((Z, Y, TB, KB), BF), V((Z, Y, TB, KB), BF), V((Z, Y, TB, KB), BF),
            V((Z, TB, KB), BF), V((Z, TB, KB), BF), V((Z, TB, KB), BF), V((Z, TB, KB), BF),
            V((2, Z, RB, HB), BF), V((2, Z, RB, HB), BF), V((2, Z, RB, HB), BF), V((2, Z, RB, HB), BF),
            V((8, RB), F32), V((TP, 8, RB), F32), V((8, HL), F32), V((FS, 8, HL), F32),
            S((n_sends,)), S((4,)), S((2, Z)), S((2, Z)), S((2, Z)), S((2, Z)), S((2, Z, Y)),
            S((Z, Y)), S((Z,)), S((Z,)), S((2, Z)), S((2, Z)), S((TP,)), S((FS,)),
        ],
        compiler_params=pltpu.CompilerParams(
            collective_id=0, has_side_effects=True, vmem_limit_bytes=60 * 1024 * 1024
        ),
        name="ffn_bwd",
    )(tokens, grad_out, up_weight, down_weight)
    ig, ug, dg, un, dn = outs
    return ig, ug, dg, un[0], dn[0]


def solution(mesh):
    fs, tp = mesh.shape["fs"], mesh.shape["tp"]
    xs = tp // 2
    zs = fs // xs

    def body(tokens, grad_out, up_weight, down_weight):
        pairs = xs == 2 and tp == 4 and zs >= 2 and up_weight.shape[1] % (128 * zs) == 0
        fits = tokens.shape[0] * zs * tokens.shape[1] * tp * 4 <= 16 * 2**20
        square = up_weight.shape[0] == up_weight.shape[1] // zs
        if pairs and fits and square:
            return fused(zs, tokens, grad_out, up_weight, down_weight)
        return on_device(tokens, grad_out, up_weight, down_weight)

    return jax.shard_map(
        body,
        mesh=mesh,
        in_specs=(P("fs", "tp"), P("fs", "tp"), P("fs", "tp"), P("tp", "fs")),
        out_specs=(P("fs", "tp"), P("fs", "tp"), P("tp", "fs"), P("fs"), P("tp")),
        check_vma=False,
    )
```

time: 419 us -> 151 us (0.36)
  waiting for transfers between devices: 352 us -> 0 us
  Pallas kernels: 0 us -> 142 us
  blocking collectives: 27.4 us -> 0 us
  matrix products: 20 us -> 0 us
  between operations: 14.2 us -> 0.64 us
  local copies, waits for them, and re-layouts: 2.22 us -> 7.65 us
    all_gather x4 -> x0, waiting for transfers between devices: 184 us -> none  [the longest x1 76.6 us: on_device(): lax.all_gather(down_weight, 'fs', axis=1, tiled=True)]
    reduce_scatter x3 -> x0, waiting for transfers between devices: 166 us -> none  [the longest x1 81.7 us: on_device(): lax.psum_scatter(lax.dot_general(cols, act, (((0,), (0,)), ((), ())), pre...]
    pallas_call x0 -> x1, Pallas kernels: none -> 142 us  [fused(): pl.pallas_call(functools.partial(kernel, Z), out_shape=(jax.ShapeDtypeStr...]
    psum x2 -> x0, blocking collectives: 27.4 us -> none  [the longest x1 20.6 us: on_device(): down_norms = lax.psum(jnp.sum(down_grad * down_grad, axis=1), 'fs')]
    dot_general x5 -> x0, matrix products: 20 us -> none  [the longest x1 4.58 us: on_device(): lax.dot_general(dpre, up_local, (((1,), (1,)), ((), ())), preferred_eleme...]
  transfers between devices with their start and end apart: 7 -> 0, of which waited for: 7 -> 0; matrix products, arithmetic and copies ran while one was open for 4% -> 0% of each run, Pallas kernels for 0% -> 0%
where the time goes in v1:
time: 151 us; the launch traced here: 150 us
  Pallas kernels  142 us (94%)
  local copies, waits for them, and re-layouts  7.65 us (5%)
    pallas_call x1, Pallas kernels, fused(): pl.pallas_call(functools.partial(kernel, Z), out_shape=(jax.ShapeDtypeStr...  142 us
    unnamed x5, local copies, waits for them, and re-layouts  5.04 us

profile of v1, /device:TPU:0, one launch (start us, length us, event | category | flops | bytes accessed | tf_op | source)
XLA Modules:
  0.0 150.4 jit_solution(17423324900169376942)
XLA Ops:
  0.6 142.1 %ffn_bwd.1 = (bf16[256,512]{1,0:T(8,128)(2,1)}, f32[256,1024]{1,0:T(8,128)}, f32[1024,256]{1,0:T(8,128)}, f32[8,256]{1,0:T(8,128)}, f32[8,1024]{1,0:T(8,128)}) custom-call(bf16[256,512]{1,0:T(8,128)(2,1)} %tok.1, bf16[256,512]{1,0:T(8,128)(2,1)} %grd.1, bf16[256,1024]{1,0:T(8,128)(2,1)} %upw.1, bf16[1024,256]{1,0:T(8,128)(2,1)} %dnw.1), custom_call_target="tpu_custom_call" | custom-call | tf_op jit(solution)/shard_map/ffn_bwd/pallas_call | solution.py:314
  142.7 1.3 slice.6
  144.0 1.4 slice.7
  145.3 1.7 %copy.12 = bf16[256,512]{1,0:T(8,128)(2,1)} copy(bf16[256,512]{1,0:T(8,128)(2,1)} %get-tuple-element.20) | data formatting | bytes 524288
  147.0 0.0 copy-start
  147.0 2.4 %copy.13 = f32[256,1024]{1,0:T(8,128)} copy(f32[256,1024]{1,0:T(8,128)} %get-tuple-element.21) | data formatting | bytes 2097152
  149.4 0.0 copy-done
  149.4 1.0 copy.14
Async XLA Ops:
  147.0 2.4 %copy-start = (f32[1024,256]{1,0:T(8,128)S(1)}, f32[1024,256]{1,0:T(8,128)}, u32[]{:S(2)}) copy-start(f32[1024,256]{1,0:T(8,128)} %get-tuple-element.22) | copy-start | bytes 3145732

commit v2 on v1

--- a/solution.py
+++ b/solution.py
@@ -58,10 +58,10 @@
     return lax.dot_general(a, b, (((ca,), (cb,)), ((), ())), preferred_element_type=F32, **kw)
 
 
-def kernel(Z, tok, grd, upw, dnw, ig_o, ug_o, dg_o, un_o, dn_o,
-           TG, UW, DW, ACT, DP, PO, PCs, PCr, PYs, PYr, PZs, PZr,
-           GXs, GXr, GZs, GZr, NUs, NUr, NDs, NDr,
-           ss, ls, wz, wx, tz, ty, tc, pc, py, pz, gx, gz, nu, nd):
+def kernel(Z, H, tok, grd, upw, dnw, ig_o, ug_o, dg_o, un_o, dn_o,
+           TG, UW, DW, ACT, DP, PO, PCs, PCr, PYs, PYr, PZs, PZr, PZd,
+           ACC, GXs, GXr, GZs, GZr, NUs, NUr, NDs, NDr,
+           ss, ls, wz, wx, tz, ty, tc, pc, py, pz, pd, gx, gz, nu, nd):
     X = Y = C = 2
     TB, KB = tok.shape
     RB = upw.shape[0]
@@ -117,8 +117,14 @@
 
     TK = (tok, grd)
 
-    def tgr(a, o, k):
-        return TG.at[a, blk(o, TB), blk(k, KB)]
+    TS = TB // H
+    pieces = [(a, h) for a in range(2) for h in range(H)]
+
+    def tgr(a, o, k, h):
+        return TG.at[a, blk(o * H + h, TS), blk(k, KB)]
+
+    def mine(a, h):
+        return TK[a].at[pl.ds(h * TS, TS), :]
 
     def w_src(a, zz):
         return upw.at[:, blk(zz, HB)] if a == 0 else dnw.at[blk(zz, HB), :]
@@ -129,46 +135,48 @@
     local = []
     for a in range(2):
         local.append(pltpu.make_async_copy(w_src(a, z), w_dst(a, f), ls.at[a]))
-        local.append(pltpu.make_async_copy(TK[a], tgr(a, z, t), ls.at[2 + a]))
+        own = TG.at[a, blk(z, TB), blk(t, KB)]
+        local.append(pltpu.make_async_copy(TK[a], own, ls.at[2 + a]))
     for d in local:
         d.start()
     pl.semaphore_wait(bar, FS - 1 + TP - 1)
 
     for a in range(2):
         send(w_src(a, z), w_dst(a, f), wx.at[a, z], DX)
-        send(TK[a], tgr(a, z, t), ty.at[a, z], DY)
-        send(TK[a], tgr(a, z, t), tc.at[a, z, y], DC)
+    for q, (a, h) in enumerate(pieces):
+        r = tgr(a, z, t, h)
+        send(mine(a, h), r, ty.at[q, z], DY)
+        send(mine(a, h), r, tc.at[q, z, y], DC)
     for i in range(1, Z):
         for a in range(2):
             send(w_src(a, order[i]), w_dst(a, f), wz.at[a, z], at_z(order[i]))
     up_z = jnp.minimum(z + 1, Z - 1)
     dn_z = jnp.maximum(z - 1, 0)
-    for a in range(2):
-        send(TK[a], tgr(a, z, t), tz.at[a, z], at_z(up_z), z < Z - 1)
-        send(TK[a], tgr(a, z, t), tz.at[a, z], at_z(dn_z), z > 0)
-
-    def arrive(i):
-        o = order[i]
-        for a in range(2):
-            r = tgr(a, o, t)
-            got(r, tz.at[a, o])
-            send(r, r, tz.at[a, o], at_z(up_z), (o < z) & (z < Z - 1))
-            send(r, r, tz.at[a, o], at_z(dn_z), (o > z) & (z > 0))
-            send(r, r, ty.at[a, o], DY)
-            send(r, r, tc.at[a, o, y], DC)
-
-    def yfwd(i):
-        o = order[i]
-        for a in range(2):
-            r = tgr(a, o, yn * C + c)
-            got(r, ty.at[a, o])
-            send(r, r, tc.at[a, o, yn], DC)
+    for q, (a, h) in enumerate(pieces):
+        r = tgr(a, z, t, h)
+        send(mine(a, h), r, tz.at[q, z], at_z(up_z), z < Z - 1)
+        send(mine(a, h), r, tz.at[q, z], at_z(dn_z), z > 0)
+
+    def arrive(i, q):
+        o = order[i]
+        r = tgr(pieces[q][0], o, t, pieces[q][1])
+        got(r, tz.at[q, o])
+        send(r, r, tz.at[q, o], at_z(up_z), (o < z) & (z < Z - 1))
+        send(r, r, tz.at[q, o], at_z(dn_z), (o > z) & (z > 0))
+        send(r, r, ty.at[q, o], DY)
+        send(r, r, tc.at[q, o, y], DC)
+
+    def yfwd(i, q):
+        o = order[i]
+        r = tgr(pieces[q][0], o, yn * C + c, pieces[q][1])
+        got(r, ty.at[q, o])
+        send(r, r, tc.at[q, o, yn], DC)
 
     def ready(i):
         o = order[i]
-        for a in range(2):
+        for q, (a, h) in enumerate(pieces):
             for yy in range(Y):
-                got(tgr(a, o, yy * C + cn), tc.at[a, o, yy])
+                got(tgr(a, o, yy * C + cn, h), tc.at[q, o, yy])
 
     def hidden(i):
         r = blk(order[i], TB)
@@ -179,29 +187,49 @@
         DP[r, :] = (dact * 2.0 * relued).astype(BF)
 
     def back(i):
-        d = DP[blk(order[i], TB), :]
+        o = order[i]
+        d = DP[blk(o, TB), :]
         for yy in range(Y):
             for cc, keep in ((cn, False), (c, True)):
                 part = dot(d, UW[blk(yy * C + cc, KB), :], 1, 1)
                 if keep:
-                    PO[i, yy] = part.astype(BF)
+                    PO[o, yy] = part.astype(BF)
                 else:
-                    PCs[i, yy] = part.astype(BF)
-                    send(PCs.at[i, yy], PCr.at[i, yy], pc.at[i, yy], DC)
+                    PCs[o, yy] = part.astype(BF)
+                    send(PCs.at[o, yy], PCr.at[o, yy], pc.at[o, yy], DC)
 
     def core_sum(i):
+        o = order[i]
         for yy in range(Y):
-            got(PCr.at[i, yy], pc.at[i, yy])
-        PYs[i] = (PO[i, yn].astype(F32) + PCr[i, yn].astype(F32)).astype(BF)
-        send(PYs.at[i], PYr.at[i], py.at[i], DY)
-
-    def y_sum(i):
-        got(PYr.at[i], py.at[i])
-        s = PO[i, y].astype(F32) + PCr[i, y].astype(F32) + PYr[i].astype(F32)
-        if i == 0:
-            return s
-        PZs[i] = s.astype(BF)
-        send(PZs.at[i], PZr.at[z], pz.at[z], at_z(order[i]))
+            got(PCr.at[o, yy], pc.at[o, yy])
+        PYs[o] = (PO[o, yn].astype(F32) + PCr[o, yn].astype(F32)).astype(BF)
+        send(PYs.at[o], PYr.at[o], py.at[o], DY)
+
+    def from_z(side, o):
+        got(PZr.at[side, o], pz.at[side, o])
+        ACC[...] += PZr[side, o].astype(F32)
+
+    def y_sum(o):
+        ACC[...] = PO[o, y].astype(F32) + PCr[o, y].astype(F32) + PYr[o].astype(F32)
+
+    def z_sum(o):
+        got(PYr.at[o], py.at[o])
+        y_sum(o)
+        pl.when((o > z) & (z > 0))(lambda: from_z(0, o))
+        pl.when((o < z) & (z < Z - 1))(lambda: from_z(1, o))
+        PZs[o] = ACC[...].astype(BF)
+        send(PZs.at[o], PZr.at[0, o], pz.at[0, o], at_z(up_z), o > z)
+        send(PZs.at[o], PZr.at[1, o], pz.at[1, o], at_z(dn_z), o < z)
+
+    def end_sum(o):
+        got(PYr.at[o], py.at[o])
+        y_sum(o)
+        PZs[o] = ACC[...].astype(BF)
+        send(PZs.at[o], PZd.at[z], pd.at[z], at_z(o), o != z)
+
+    def from_end(zz):
+        got(PZd.at[zz], pd.at[zz])
+        ACC[...] += PZd[zz].astype(F32)
 
     def grads(a, ff):
         if a == 0:
@@ -214,8 +242,11 @@
             r = w_dst(a, o * X + x)
             got(r, wz.at[a, o])
             send(r, r, wx.at[a, o], DX)
-    yfwd(0)
-    arrive(1)
+    every = range(len(pieces))
+    for q in every:
+        yfwd(0, q)
+    for q in every:
+        arrive(1, q)
     for d in local:
         d.wait()
     for i in range(Z):
@@ -225,14 +256,14 @@
         ready(i)
         hidden(i)
         if i + 1 < Z:
+            for q in every:
+                yfwd(i + 1, q)
+                if i + 2 < Z:
+                    arrive(i + 2, q)
+            if i + 2 == Z:
+                for j in range(i):
+                    core_sum(j)
             back(i)
-            yfwd(i + 1)
-        if i + 2 < Z:
-            arrive(i + 2)
-        if i >= 1:
-            core_sum(i - 1)
-        if i >= 2 and i + 1 < Z:
-            y_sum(i - 1)
 
     far = list(range(Z - 1, -1, -1))
     for i in far:
@@ -240,9 +271,9 @@
             GXs[a, i] = grads(a, order[i] * X + xn).astype(BF)
             send(GXs.at[a, i], GXr.at[a, i], gx.at[a, i], DX)
     back(Z - 1)
-    if Z > 2:
-        y_sum(Z - 2)
-    for i in far:
+    for i in range(max(Z - 2, 0), Z):
+        core_sum(i)
+    for j, i in enumerate(far):
         o = order[i]
         for a in range(2):
             g = grads(a, o * X + x)
@@ -255,14 +286,18 @@
                 ug_o[:, blk(o, HB)] = g
             else:
                 dg_o[blk(o, HB), :] = g
-        if i == Z - 1:
-            core_sum(Z - 1)
-    y_sum(Z - 1)
-    total = y_sum(0)
-    for i in range(1, Z):
-        got(PZr.at[order[i]], pz.at[order[i]])
-        total = total + PZr[order[i]].astype(F32)
-    ig_o[...] = total.astype(BF)
+        if j == 0:
+            end_sum(jnp.int32(Z - 1))
+            end_sum(jnp.int32(0))
+    for o in range(1, Z - 1):
+        z_sum(jnp.int32(o))
+    y_sum(z)
+    inner = (z > 0) & (z < Z - 1)
+    pl.when(inner)(lambda: from_z(0, z))
+    pl.when(inner)(lambda: from_z(1, z))
+    for zz in range(Z):
+        pl.when((z == 0) & (zz > 0) | (z == Z - 1) & (zz < Z - 1))(functools.partial(from_end, zz))
+    ig_o[...] = ACC[...].astype(BF)
 
     for i in range(1, Z):
         o = order[i]
@@ -290,14 +325,23 @@
     for p in range(1, FS):
         q = (f + p) % FS
         got(NDr.at[q], nd.at[q])
-    un_o[...] = sum(NUr[q] for q in range(TP))
-    dn_o[...] = sum(NDr[q] for q in range(FS))
+    un_o[...] = sum(NUr[q] for q in range(TP))[0:1, :]
+    dn_o[...] = sum(NDr[q] for q in range(FS))[0:1, :]
 
     for d, cond in sends:
         if cond is None:
             d.wait_send()
         else:
             pl.when(cond)(d.wait_send)
+
+
+def hand_over(*refs):
+    n = len(refs) // 2
+    copies = [pltpu.make_async_copy(refs[i], refs[n + i], refs[-1].at[i]) for i in range(n)]
+    for d in copies:
+        d.start()
+    for d in copies:
+        d.wait()
 
 
 def fused(Z, tokens, grad_out, up_weight, down_weight):
@@ -309,35 +353,43 @@
     V, S = pltpu.VMEM, pltpu.SemaphoreType.DMA
     any_ = pl.BlockSpec(memory_space=pl.ANY)
     vm = pl.BlockSpec(memory_space=pltpu.VMEM)
-    n_sends = 2 * 3 + 2 * (Z - 1) + 4 + 8 * (Z - 1) + 2 * Z + 2 * (Z - 1)
-    n_sends += 2 * Z + Z + Z - 1 + 2 * Z + 2 * (Z - 1) + TP - 1 + FS - 1
+    H = 2
+    n_sends = 48 * Z
     outs = pl.pallas_call(
-        functools.partial(kernel, Z),
+        functools.partial(kernel, Z, H),
         out_shape=(
             jax.ShapeDtypeStruct((TB, KB), BF),
             jax.ShapeDtypeStruct((RB, HL), F32),
             jax.ShapeDtypeStruct((HL, RB), F32),
-            jax.ShapeDtypeStruct((8, RB), F32),
-            jax.ShapeDtypeStruct((8, HL), F32),
+            jax.ShapeDtypeStruct((1, RB), F32),
+            jax.ShapeDtypeStruct((1, HL), F32),
         ),
         in_specs=[any_] * 4,
         out_specs=[vm] * 5,
         scratch_shapes=[
             V((2, T, D), BF), V((D, HB), BF), V((HB, D), BF), V((T, HB), BF), V((T, HB), BF),
             V((Z, Y, TB, KB), BF), V((Z, Y, TB, KB), BF), V((Z, Y, TB, KB), BF),
-            V((Z, TB, KB), BF), V((Z, TB, KB), BF), V((Z, TB, KB), BF), V((Z, TB, KB), BF),
+            V((Z, TB, KB), BF), V((Z, TB, KB), BF), V((Z, TB, KB), BF), V((2, Z, TB, KB), BF), V((Z, TB, KB), BF), V((TB, KB), F32),
             V((2, Z, RB, HB), BF), V((2, Z, RB, HB), BF), V((2, Z, RB, HB), BF), V((2, Z, RB, HB), BF),
             V((8, RB), F32), V((TP, 8, RB), F32), V((8, HL), F32), V((FS, 8, HL), F32),
-            S((n_sends,)), S((4,)), S((2, Z)), S((2, Z)), S((2, Z)), S((2, Z)), S((2, Z, Y)),
-            S((Z, Y)), S((Z,)), S((Z,)), S((2, Z)), S((2, Z)), S((TP,)), S((FS,)),
+            S((n_sends,)), S((4,)), S((2, Z)), S((2, Z)), S((2 * H, Z)), S((2 * H, Z)), S((2 * H, Z, Y)),
+            S((Z, Y)), S((Z,)), S((2, Z)), S((Z,)), S((2, Z)), S((2, Z)), S((TP,)), S((FS,)),
         ],
         compiler_params=pltpu.CompilerParams(
-            collective_id=0, has_side_effects=True, vmem_limit_bytes=60 * 1024 * 1024
+            collective_id=0, has_side_effects=True, vmem_limit_bytes=40 * 2**20
         ),
         name="ffn_bwd",
     )(tokens, grad_out, up_weight, down_weight)
-    ig, ug, dg, un, dn = outs
-    return ig, ug, dg, un[0], dn[0]
+    ig, ug, dg, un, dn = pl.pallas_call(
+        hand_over,
+        out_shape=tuple(jax.ShapeDtypeStruct(o.shape, o.dtype) for o in outs),
+        in_specs=[vm] * 5,
+        out_specs=[any_] * 5,
+        scratch_shapes=[S((5,))],
+        compiler_params=pltpu.CompilerParams(vmem_limit_bytes=8 * 2**20),
+        name="hand_over",
+    )(*outs)
+    return ig, ug, dg, un.reshape(RB), dn.reshape(HL)
 
 
 def solution(mesh):

time: 151 us -> 142 us (0.940)
  Pallas kernels: 142 us -> 137 us
  local copies, waits for them, and re-layouts: 7.65 us -> 3.97 us
    pallas_call x1 -> x2, Pallas kernels: 142 us -> 137 us  [the longest x1 135 us: fused(): pl.pallas_call(functools.partial(kernel, Z, H), out_shape=(jax.ShapeDtype...]
    slice x2 -> x0, local copies, waits for them, and re-layouts: 2.61 us -> none  [fused(): return (ig, ug, dg, un[0], dn[0])]
    unnamed x5 -> x8, local copies, waits for them, and re-layouts: 5.04 us -> 3.97 us
where the time goes in v2:
time: 142 us
  Pallas kernels  137 us (96%)
  local copies, waits for them, and re-layouts  3.97 us (3%)
    pallas_call x1, Pallas kernels, fused(): pl.pallas_call(functools.partial(kernel, Z, H), out_shape=(jax.ShapeDtype...  135 us
    unnamed x8, local copies, waits for them, and re-layouts  3.97 us

profile of v2, /device:TPU:0, one launch (start us, length us, event | category | flops | bytes accessed | tf_op | source)
XLA Modules:
  0.0 141.6 jit_solution(6985012323209450223)
XLA Ops:
  0.6 0.0 copy-start
  0.6 1.0 copy-done
  1.7 0.0 copy-start.1
  1.7 1.0 copy-done.1
  2.7 0.0 copy-start.2
  2.7 0.9 copy-done.2
  3.7 0.0 copy-start.3
  3.7 0.9 copy-done.3
  4.6 135.4 %ffn_bwd.1 = (bf16[256,512]{1,0:T(8,128)(2,1)S(1)}, f32[256,1024]{1,0:T(8,128)S(1)}, f32[1024,256]{1,0:T(8,128)S(1)}, f32[1,256]{1,0:T(1,128)S(1)}, f32[1,1024]{1,0:T(1,128)S(1)}) custom-call(bf16[256,512]{1,0:T(8,128)(2,1)S(1)} %copy-done.2, bf16[256,512]{1,0:T(8,128)(2,1)S(1)} %copy-done.3, bf16[256,1024]{1,0:T(8,128)(2,1)S(1)} %copy-done, ...), custom_call_target="tpu_custom_call" | custom-call | tf_op jit(solution)/shard_map/ffn_bwd/pallas_call | solution.py:358
  140.0 1.5 %hand_over.1 = (bf16[256,512]{1,0:T(8,128)(2,1)}, f32[256,1024]{1,0:T(8,128)}, f32[1024,256]{1,0:T(8,128)}, f32[1,256]{1,0:T(1,128)}, f32[1,1024]{1,0:T(1,128)}) custom-call(bf16[256,512]{1,0:T(8,128)(2,1)S(1)} %get-tuple-element.15.refs_0_, f32[256,1024]{1,0:T(8,128)S(1)} %get-tuple-element.16.refs_1_, f32[1024,256]{1,0:T(8,128)S(1)} %get-tuple-element.17.refs_2_, ...), custom_call_target="tpu_custom_call" | custom-call | tf_op jit(solution)/shard_map/hand_over/pallas_call | solution.py:383
Async XLA Ops:
  0.6 1.0 copy-start
  1.7 1.0 copy-start.1
  2.7 0.9 copy-start.2
  3.7 0.9 copy-start.3
